TPU v7x, 32 devices: a whole 2x2x4 slice. The times are simulated.
32 devices in a mesh: rep: 2 (over x), fs: 8 (over z, y), tp: 2 (over core).
Axes of the slice: x: 2, y: 2, z: 4, core: 2. Of those that a mesh axis runs over, the one named last changes fastest.
Arguments:
- hidden_in: bfloat16 [12288, 2048], P(('rep', 'fs', 'tp')), may hold values from -6 to 6
- norm_gain: float32 [2048], replicated, may hold values from 0.1 to 1.9
- up_weight: float32 [2048, 8192], P('fs', 'tp'), may hold values from -0.125 to 0.125
- up_scale: float32 [8192], P('tp'), may hold values from 0.5 to 2
- down_weight: float32 [8192, 2048], P('tp', 'fs'), may hold values from -0.0625 to 0.0625
- down_scale: float32 [2048], replicated, may hold values from 0.5 to 2
Outputs:
- layer_out: bfloat16 [12288, 2048], P(('rep', 'fs', 'tp'))
All inputs are finite; a program needn't handle non-finite values.
Results may differ from a plain program's by a relative error of at most 0.0085.
Values may be sent and summed in bfloat16 or wider, within the bound.
A program may use at most 128 MiB of HBM per device.

v0:
```python
import jax
import jax.numpy as jnp
from jax import lax
from jax.sharding import PartitionSpec as P


def body(hidden_in, norm_gain, up_weight, up_scale, down_weight, down_scale):
    rows = hidden_in.astype(jnp.float32)
    normed = (
        rows * lax.rsqrt(jnp.mean(rows * rows, axis=1, keepdims=True) + 1e-06) * norm_gain
    ).astype(jnp.bfloat16)
    gathered = lax.all_gather(normed, "tp", axis=0, tiled=True)
    up_low = up_weight.astype(jnp.bfloat16)
    down_low = down_weight.astype(jnp.bfloat16)
    up_whole = lax.all_gather(up_low, "fs", axis=0, tiled=True)
    pre = jnp.dot(gathered, up_whole, preferred_element_type=jnp.float32)
    down_whole = lax.all_gather(down_low, "fs", axis=1, tiled=True)
    act = jnp.square(jnp.maximum(pre * up_scale, 0.0)).astype(jnp.bfloat16)
    summed = lax.psum_scatter(
        jnp.dot(act, down_whole, preferred_element_type=jnp.float32).astype(jnp.bfloat16),
        "tp",
        scatter_dimension=0,
        tiled=True,
    ).astype(jnp.float32)
    return (summed * down_scale).astype(jnp.bfloat16)


def solution(mesh):
    placed = (P(("rep", "fs", "tp"), None), P(), P("fs", "tp"), P("tp"), P("tp", "fs"), P())
    return jax.shard_map(
        body, mesh=mesh, in_specs=placed, out_specs=P(("rep", "fs", "tp"), None), check_vma=False
    )
```

profile of v0, /device:TPU:0, one launch (start us, length us, event | category | flops | bytes accessed | tf_op | source)
XLA Modules:
  0.0 542.0 jit_solution(9499222584294802348)
XLA Ops:
  6.5 0.0 all-gather.4.cloned.1.call-start
  6.5 1.8 fusion
  8.3 3.0 fusion.2
  11.3 0.0 all-gather.4.cloned.1.call-update
  11.3 0.0 all-gather.6.cloned.1.call-start
  11.4 3.8 convert_element_type.26
  15.2 0.0 all-gather.6.cloned.1.call-update
  15.3 0.0 copy-start.1
  15.3 0.0 all-gather.8.cloned.1.call-start
  15.3 3.7 convert_element_type.28
  19.0 0.0 all-gather.8.cloned.1.call-update
  19.1 0.0 reduce-scatter.2.cloned.1.call-start
  19.1 7.2 %all-gather.4.cloned.1.call-done = bf16[768,2048]{1,0:T(8,128)(2,1)} async-done(((bf16[384,2048]{1,0:T(8,128)(2,1)}), bf16[768,2048]{1,0:T(8,128)(2,1)}) %all-gather.4.cloned.1.call-update) | async-done | bytes 3145744 | tf_op jit(solution)/shard_map/all_gather | solution.py:12
  26.3 230.6 %all-gather.6.cloned.1.call-done = bf16[2048,4096]{1,0:T(8,128)(2,1)} async-done(((bf16[256,4096]{1,0:T(8,128)(2,1)}), bf16[2048,4096]{1,0:T(8,128)(2,1)}) %all-gather.6.cloned.1.call-update) | async-done | bytes 16777232 | tf_op jit(solution)/shard_map/all_gather | solution.py:15
  257.0 227.6 %all-gather.8.cloned.1.call-done = bf16[4096,2048]{1,0:T(8,128)(2,1)} async-done(((bf16[4096,256]{1,0:T(8,128)(2,1)}), bf16[4096,2048]{1,0:T(8,128)(2,1)}) %all-gather.8.cloned.1.call-update) | async-done | bytes 16777232 | tf_op jit(solution)/shard_map/all_gather | solution.py:17
  484.5 0.0 copy-done.1
  484.5 38.5 %convolution_convert_fusion = bf16[768,2048]{1,0:T(8,128)(2,1)} fusion(bf16[4096,2048]{1,0:T(8,128)(2,1)} %all-gather.8.cloned.1.call-done, bf16[768,2048]{1,0:T(8,128)(2,1)} %all-gather.4.cloned.1.call-done, bf16[2048,4096]{1,0:T(8,128)(2,1)} %all-gather.6.cloned.1.call-done, f32[4096]{0:T(1024)S(1)} %copy-done.1), kind=kOutput, calls=%fused_computation.3 | convolution fusion | flops 25783959552 | bytes 39862272 | tf_op jit(solution)/shard_map/dot_general | solution.py:20
  523.0 0.0 copy-start
  523.0 0.0 reduce-scatter.2.cloned.1.call-update
  523.0 9.5 %reduce-scatter.2.cloned.1.call-done = bf16[384,2048]{1,0:T(8,128)(2,1)} async-done(((bf16[768,2048]{1,0:T(8,128)(2,1)}), bf16[384,2048]{1,0:T(8,128)(2,1)}) %reduce-scatter.2.cloned.1.call-update) | async-done | bytes 1572880 | tf_op jit(solution)/shard_map/reduce_scatter | solution.py:19
  532.6 0.0 copy-done
  532.6 2.9 multiply_convert_fusion.1
  (1 shorter events, 0.0 us)
Async XLA Ops:
  6.5 19.8 %all-gather.4.cloned.1.call-start = ((), (), s32[]{:S(2)}) async-start(), calls=%async_computation.1 | async-start | bytes 4718592 | tf_op jit(solution)/shard_map/all_gather | solution.py:12
  11.3 245.6 %all-gather.6.cloned.1.call-start = ((), (), s32[]{:S(2)}) async-start(), calls=%async_computation.2 | async-start | bytes 18874368 | tf_op jit(solution)/shard_map/all_gather | solution.py:15
  15.3 469.3 %copy-start.1 = (f32[4096]{0:T(1024)S(1)}, f32[4096]{0:T(1024)}, u32[]{:S(2)}) copy-start(f32[4096]{0:T(1024)} %param.9) | copy-start | bytes 49156
  15.3 469.3 %all-gather.8.cloned.1.call-start = ((), (), s32[]{:S(2)}) async-start(), calls=%async_computation.3 | async-start | bytes 18874368 | tf_op jit(solution)/shard_map/all_gather | solution.py:17
  19.1 513.5 %reduce-scatter.2.cloned.1.call-start = ((), (), s32[]{:S(2)}) async-start(), calls=%async_computation.4 | async-start | bytes 4718592 | tf_op jit(solution)/shard_map/reduce_scatter | solution.py:19
  523.0 9.5 %copy-start = (f32[2048]{0:T(1024)S(1)}, f32[2048]{0:T(1024)}, u32[]{:S(2)}) copy-start(f32[2048]{0:T(1024)} %param.11) | copy-start | bytes 24580
Sparse Core Ops, SparseCore 0:
  11.5 14.8 all-gather.3
  28.5 228.4 all-gather.5
  259.0 225.4 all-gather.7
  523.2 9.3 reduce-scatter.1
where the time goes:
time: 542 us
  waiting for transfers between devices  475 us (88%)
  matrix products  38.5 us (7%)
  other arithmetic  15.3 us (3%)
  between operations  13.1 us (2%)
    all_gather x1, waiting for transfers between devices, body(): up_whole = lax.all_gather(up_low, 'fs', axis=0, tiled=True)  231 us
    all_gather x1, waiting for transfers between devices, body(): down_whole = lax.all_gather(down_low, 'fs', axis=1, tiled=True)  228 us
    dot_general x1, matrix products, body(): jnp.dot(act, down_whole, preferred_element_type=jnp.float32)  38.5 us
  transfers between devices with their start and end apart: 4, of which 4 were waited for; matrix products, arithmetic and copies ran while one was open for 1% of the time, Pallas kernels for 0%

commit v1 on v0

v1 whole, which is shorter than its diff:
```python
import jax
import jax.numpy as jnp
from jax import lax
from jax.sharding import Mesh, PartitionSpec as P


def body(hidden_in, norm_gain, up_weight, up_scale, down_weight, down_scale):
    rep, pair = lax.axis_index("rep"), lax.axis_index("fy")
    n_rep, n_pair = lax.axis_size("rep"), lax.axis_size("fy")
    group = ("rep", "fy", "tp")
    units = up_weight.shape[1] // n_rep

    rows = hidden_in.astype(jnp.float32)
    normed = (
        rows * lax.rsqrt(jnp.mean(rows * rows, axis=1, keepdims=True) + 1e-06) * norm_gain
    ).astype(jnp.bfloat16)
    up_low = lax.dynamic_slice_in_dim(up_weight, rep * units, units, 1).astype(jnp.bfloat16)
    up_pair = lax.all_to_all(up_low, "fy", 1, 0, tiled=True)
    up_whole = lax.all_gather(up_pair, "fz", axis=0, tiled=True)
    gathered = lax.all_gather(normed, group, axis=0, tiled=True)
    down_low = lax.dynamic_slice_in_dim(down_weight, rep * units, units, 0).astype(jnp.bfloat16)
    down_pair = lax.all_to_all(down_low, "fy", 0, 1, tiled=True)
    down_whole = lax.all_gather(down_pair, "fz", axis=1, tiled=True)
    width = units // n_pair
    scale = lax.dynamic_slice_in_dim(up_scale, (rep * n_pair + pair) * width, width, 0)
    pre = jnp.dot(gathered, up_whole, preferred_element_type=jnp.float32)
    act = jnp.square(jnp.maximum(pre * scale, 0.0)).astype(jnp.bfloat16)
    summed = lax.psum_scatter(
        jnp.dot(act, down_whole, preferred_element_type=jnp.float32).astype(jnp.bfloat16),
        group,
        scatter_dimension=0,
        tiled=True,
    ).astype(jnp.float32)
    return (summed * down_scale).astype(jnp.bfloat16)


def solution(mesh):
    n_rep, n_fs, n_tp = (mesh.shape[a] for a in ("rep", "fs", "tp"))
    pair = 2 if n_fs % 2 == 0 else 1
    split = Mesh(
        mesh.devices.reshape(n_rep, n_fs // pair, pair, n_tp), ("rep", "fz", "fy", "tp")
    )
    fs = ("fz", "fy")
    tokens = P(("rep", *fs, "tp"), None)
    placed = (tokens, P(), P(fs, "tp"), P("tp"), P("tp", fs), P())
    return jax.shard_map(body, mesh=split, in_specs=placed, out_specs=tokens, check_vma=False)
```

time: 542 us -> 398 us (0.73)
  waiting for transfers between devices: 475 us -> 306 us
  blocking collectives: 0 us -> 32.8 us
  other arithmetic: 15.3 us -> 4.9 us
  local copies, waits for them, and re-layouts: 0.01 us -> 7.39 us
    all_gather x3, waiting for transfers between devices: 465 us -> 213 us  [the longest x1 80.8 us: body(): down_whole = lax.all_gather(down_pair, 'fz', axis=1, tiled=True)]
    reduce_scatter x1, waiting for transfers between devices: 9.52 us -> 92.4 us  [body(): lax.psum_scatter(jnp.dot(act, down_whole, preferred_element_type=jnp.floa...]
    all_to_all x0 -> x2, blocking collectives: none -> 32.8 us  [the longest x1 17.7 us: body(): up_pair = lax.all_to_all(up_low, 'fy', 1, 0, tiled=True)]
    convert_element_type x2 -> x0, other arithmetic: 7.54 us -> none  [the longest x1 3.83 us: body(): up_low = up_weight.astype(jnp.bfloat16)]
where the time goes in v1:
time: 398 us; the launch traced here: 397 us
  waiting for transfers between devices  306 us (77%)
  matrix products  33.1 us (8%)
  blocking collectives  32.8 us (8%)
  between operations  13.2 us (3%)
  local copies, waits for them, and re-layouts  7.39 us (2%)
  other arithmetic  4.9 us (1%)
    reduce_scatter x1, waiting for transfers between devices, body(): lax.psum_scatter(jnp.dot(act, down_whole, preferred_element_type=jnp.floa...  92.4 us
    all_gather x1, waiting for transfers between devices, body(): down_whole = lax.all_gather(down_pair, 'fz', axis=1, tiled=True)  80.8 us
    all_gather x1, waiting for transfers between devices, body(): gathered = lax.all_gather(normed, group, axis=0, tiled=True)  72.4 us
    all_gather x1, waiting for transfers between devices, body(): up_whole = lax.all_gather(up_pair, 'fz', axis=0, tiled=True)  60.1 us
    dot_general x1, matrix products, body(): jnp.dot(act, down_whole, preferred_element_type=jnp.float32)  33.1 us
    all_to_all x1, blocking collectives, body(): up_pair = lax.all_to_all(up_low, 'fy', 1, 0, tiled=True)  17.7 us
    all_to_all x1, blocking collectives, body(): down_pair = lax.all_to_all(down_low, 'fy', 0, 1, tiled=True)  15.2 us
  transfers between devices with their start and end apart: 4, of which 4 were waited for; matrix products, arithmetic and copies ran while one was open for 1% of the time, Pallas kernels for 0%

profile of v1, /device:TPU:0, one launch (start us, length us, event | category | flops | bytes accessed | tf_op | source)
XLA Modules:
  0.0 397.5 jit_solution(277988505916214377)
XLA Ops:
  6.5 0.0 all-gather.6.cloned.1.call-start
  6.5 1.7 constant_dynamic-slice_fusion
  8.3 0.5 copy.10
  8.8 17.7 %all_to_all.38 = bf16[256,2,1024]{0,2,1:T(8,128)(2,1)S(1)} all-to-all(bf16[256,2,1024]{0,2,1:T(8,128)(2,1)S(1)} %bitcast.21), channel_id=1, replica_groups=mesh['rep'=2,'fz'=4,'fy'=2,'tp'=2] {'fy'}, dimensions={1} | all-to-all | bytes 2097152 | tf_op jit(solution)/shard_map/all_to_all | solution.py:18
  26.5 1.3 copy.8
  27.8 0.0 copy-start
  27.8 0.0 all-gather.6.cloned.1.call-update
  27.8 0.0 copy-start.1
  27.8 0.0 all-gather.8.cloned.1.call-start
  27.9 1.8 dynamic-slice_convert_fusion
  29.7 15.2 %all_to_all.39 = bf16[2,1024,256]{2,1,0:T(8,128)(2,1)S(1)} all-to-all(bf16[2,1024,256]{2,1,0:T(8,128)(2,1)S(1)} %bitcast.18), channel_id=1, replica_groups=mesh['rep'=2,'fz'=4,'fy'=2,'tp'=2] {'fy'}, dimensions={0} | all-to-all | bytes 2097152 | tf_op jit(solution)/shard_map/all_to_all | solution.py:22
  44.9 1.3 copy.9
  46.2 0.0 all-gather.8.cloned.1.call-update
  46.2 0.0 all-gather.4.cloned.1.call-start
  46.2 0.0 copy-done
  46.3 0.4 fusion
  46.7 0.0 copy-done.1
  46.7 1.6 fusion.2
  48.2 0.0 all-gather.4.cloned.1.call-update
  48.3 0.0 reduce-scatter.2.cloned.1.call-start
  48.3 0.7 dynamic_slice.10
  49.0 60.1 %all-gather.6.cloned.1.call-done = bf16[2048,1024]{1,0:T(8,128)(2,1)} async-done(((bf16[512,1024]{1,0:T(8,128)(2,1)}), bf16[2048,1024]{1,0:T(8,128)(2,1)}) %all-gather.6.cloned.1.call-update) | async-done | bytes 4194320 | tf_op jit(solution)/shard_map/all_gather | solution.py:19
  109.2 80.8 %all-gather.8.cloned.1.call-done = bf16[1024,2048]{0,1:T(8,128)(2,1)} async-done(((bf16[1024,512]{0,1:T(8,128)(2,1)}), bf16[1024,2048]{0,1:T(8,128)(2,1)}) %all-gather.8.cloned.1.call-update) | async-done | bytes 4194320 | tf_op jit(solution)/shard_map/all_gather | solution.py:23
  190.0 72.4 %all-gather.4.cloned.1.call-done = bf16[3072,2048]{1,0:T(8,128)(2,1)} async-done(((bf16[384,2048]{1,0:T(8,128)(2,1)}), bf16[3072,2048]{1,0:T(8,128)(2,1)}) %all-gather.4.cloned.1.call-update) | async-done | bytes 12582928 | tf_op jit(solution)/shard_map/all_gather | solution.py:20
  262.4 33.1 %convolution_convert_fusion = bf16[3072,2048]{1,0:T(8,128)(2,1)} fusion(bf16[1024,2048]{0,1:T(8,128)(2,1)} %all-gather.8.cloned.1.call-done, bf16[3072,2048]{1,0:T(8,128)(2,1)} %all-gather.4.cloned.1.call-done, bf16[2048,1024]{1,0:T(8,128)(2,1)} %all-gather.6.cloned.1.call-done, f32[1024]{0:T(1024)S(1)} %dynamic_slice.10), kind=kOutput, calls=%fused_computation.1 | convolution fusion | flops 25788678144 | bytes 33558528 | tf_op jit(solution)/shard_map/dot_general | solution.py:29
  295.5 0.0 copy-start.2
  295.5 0.0 reduce-scatter.2.cloned.1.call-update
  295.5 92.4 %reduce-scatter.2.cloned.1.call-done = bf16[384,2048]{1,0:T(8,128)(2,1)} async-done(((bf16[3072,2048]{1,0:T(8,128)(2,1)}), bf16[384,2048]{1,0:T(8,128)(2,1)}) %reduce-scatter.2.cloned.1.call-update) | async-done | bytes 1572880 | tf_op jit(solution)/shard_map/reduce_scatter | solution.py:28
  388.0 0.0 copy-done.2
  388.0 2.9 multiply_convert_fusion.1
  (1 shorter events, 0.0 us)
Async XLA Ops:
  6.5 102.6 %all-gather.6.cloned.1.call-start = ((), (), s32[]{:S(2)}) async-start(), calls=%async_computation.4 | async-start | bytes 5242880 | tf_op jit(solution)/shard_map/all_gather | solution.py:19
  27.8 18.5 %copy-start = (bf16[384,2048]{1,0:T(8,128)(2,1)S(1)}, bf16[384,2048]{1,0:T(8,128)(2,1)}, u32[]{:S(2)}) copy-start(bf16[384,2048]{1,0:T(8,128)(2,1)} %param.6) | copy-start | bytes 4718596
  27.8 18.8 %copy-start.1 = (f32[2048]{0:T(1024)S(1)}, f32[2048]{0:T(1024)}, u32[]{:S(2)}) copy-start(f32[2048]{0:T(1024)} %param.7) | copy-start | bytes 24580
  27.8 162.1 %all-gather.8.cloned.1.call-start = ((), (), s32[]{:S(2)}) async-start(), calls=%async_computation.5 | async-start | bytes 5242880 | tf_op jit(solution)/shard_map/all_gather | solution.py:23
  46.2 216.2 %all-gather.4.cloned.1.call-start = ((), (), s32[]{:S(2)}) async-start(), calls=%async_computation.3 | async-start | bytes 14155776 | tf_op jit(solution)/shard_map/all_gather | solution.py:20
  48.3 339.7 %reduce-scatter.2.cloned.1.call-start = ((), (), s32[]{:S(2)}) async-start(), calls=%async_computation.6 | async-start | bytes 14155776 | tf_op jit(solution)/shard_map/reduce_scatter | solution.py:28
  295.5 92.5 %copy-start.2 = (f32[2048]{0:T(1024)S(1)}, f32[2048]{0:T(1024)}, u32[]{:S(2)}) copy-start(f32[2048]{0:T(1024)} %param.11) | copy-start | bytes 24580
Sparse Core Ops, SparseCore 0:
  27.9 81.1 all-gather.5
  110.7 79.2 all-gather.7
  191.9 70.4 all-gather.3
  295.7 92.2 reduce-scatter.1

commit v2 on v1

v2 whole, which is shorter than its diff:
```python
import functools

import jax
import jax.numpy as jnp
from jax import lax
from jax.experimental import pallas as pl
from jax.experimental.pallas import tpu as pltpu
from jax.sharding import Mesh, PartitionSpec as P

MESH = pl.DeviceIdType.MESH


def kernel(
    n, normed, up_own, up_peer, dn_own, dn_peer, up_scale, dn_scale, out,
    tok, up_w, dn_w, act, psend, precv, csum, ra1, rb1, ra2, rb2, ss, rs, ls,
):
    x, z, y, c = (lax.axis_index(a) for a in ("rep", "fz", "fy", "tp"))
    ox, oy, oc = 1 - x, 1 - y, 1 - c
    right, left = lax.rem(z + 1, n), lax.rem(z + n - 1, n)
    to_x, to_y, to_c = {"rep": ox}, {"fy": oy}, {"tp": oc}
    to_right, to_left = {"fz": right}, {"fz": left}
    kr, width = up_own.shape
    rows, depth = normed.shape
    half = depth // 2
    top = rows // 2

    barrier = pltpu.get_barrier_semaphore()
    for other in (to_x, to_y, to_c, to_right, to_left):
        pl.semaphore_signal(barrier, inc=1, device_id=other, device_id_type=MESH)
    pl.semaphore_wait(barrier, 5)

    copies = []

    def send(src, dst, other):
        i = len(copies)
        copy = pltpu.make_async_remote_copy(
            src_ref=src, dst_ref=dst, send_sem=ss.at[i], recv_sem=rs.at[i],
            device_id=other, device_id_type=MESH,
        )
        copy.start()
        copies.append(copy)
        return copy

    def up_at(zz, yy):
        return up_w.at[pl.ds(pl.multiple_of((zz * 2 + yy) * kr, kr), kr)]

    def dn_at(zz, yy):
        return dn_w.at[zz * 2 + yy]

    ring = {}

    def hop(step, yy, chain):
        if step == 0 and chain == 0:
            u_src, d_src = up_own, dn_own
        else:
            u_src = up_at(lax.rem(z - step + n, n), yy)
            d_src = dn_at(lax.rem(z + step, n), yy)
        ring[chain, step] = (
            send(u_src, up_at(lax.rem(z - step + n, n), yy), to_right),
            send(d_src, dn_at(lax.rem(z + step, n), yy), to_left),
        )

    def arrived(step, chain):
        for copy in ring[chain, step]:
            copy.wait_recv()

    hop(0, y, 0)
    y_up = send(up_peer, up_at(z, y), to_y)
    y_dn = send(dn_peer, dn_at(z, y), to_y)
    tx = send(normed, tok.at[c, x, y], to_x)
    ty = send(normed, tok.at[c, x, y], to_y)
    tc = send(normed, tok.at[c, x, y], to_c)
    mine = (
        pltpu.make_async_copy(up_own, up_at(z, y), ls.at[0]),
        pltpu.make_async_copy(dn_own, dn_at(z, y), ls.at[1]),
        pltpu.make_async_copy(normed, tok.at[c, x, y], ls.at[2]),
    )
    for copy in mine:
        copy.start()

    arrived(0, 0)
    hop(1, y, 0)
    y_up.wait_recv()
    y_dn.wait_recv()
    hop(0, oy, 1)
    for step in range(1, n - 2):
        arrived(step, 0)
        hop(step + 1, y, 0)
    tx.wait_recv()
    diag_y = send(tok.at[c, ox, y, pl.ds(0, top)], tok.at[c, ox, y, pl.ds(0, top)], to_y)
    cx = send(tok.at[c, ox, y], tok.at[c, ox, y], to_c)
    arrived(0, 1)
    hop(1, oy, 1)
    ty.wait_recv()
    diag_x = send(tok.at[c, x, oy, pl.ds(top, top)], tok.at[c, x, oy, pl.ds(top, top)], to_x)
    cy = send(tok.at[c, x, oy], tok.at[c, x, oy], to_c)
    for step in range(1, n - 2):
        arrived(step, 1)
        hop(step + 1, oy, 1)
    diag_y.wait_recv()
    diag_x.wait_recv()
    cd = send(tok.at[c, ox, oy], tok.at[c, ox, oy], to_c)
    arrived(n - 2, 0)
    arrived(n - 2, 1)
    for copy in (tc, cx, cy, cd):
        copy.wait_recv()
    for copy in mine:
        copy.wait()

    tile = min(256, width)
    n_fs, _, cols = dn_w.shape
    per_half = n_fs // 2

    def hidden(cc, xx, yy):
        @pl.loop(0, width // tile)
        def _(i):
            at = pl.ds(pl.multiple_of(i * tile, tile), tile)
            pre = jnp.dot(tok[cc, xx, yy], up_w[:, at], preferred_element_type=jnp.float32)
            act[:, at] = jnp.square(jnp.maximum(pre * up_scale[:, at], 0.0)).astype(jnp.bfloat16)

    def each_slot(emit):
        for h in range(2):
            def one(s, at):
                part = jnp.dot(
                    act[...], dn_w[h * per_half + s], preferred_element_type=jnp.float32
                )
                emit(h, at, part.astype(jnp.bfloat16))

            if cols % 128 == 0:
                @pl.loop(0, per_half)
                def _(s):
                    one(s, pl.ds(pl.multiple_of(s * cols, cols), cols))
            else:
                for s in range(per_half):
                    one(s, pl.ds(s * cols, cols))

    def for_partner(xx, yy):
        hidden(oc, xx, yy)

        def emit(h, at, part):
            psend[xx, yy, h, :, at] = part

        each_slot(emit)
        return send(psend.at[xx, yy], precv.at[xx, yy], to_c)

    def for_own(xx, yy, got):
        hidden(c, xx, yy)
        got.wait_recv()

        def emit(h, at, part):
            total = part.astype(jnp.float32) + precv[xx, yy, h, :, at].astype(jnp.float32)
            csum[xx, yy, h, :, at] = total.astype(jnp.bfloat16)

        each_slot(emit)

    def add(xx, yy, h, got):
        total = csum[xx, yy, h].astype(jnp.float32) + got[...].astype(jnp.float32)
        csum[xx, yy, h] = total.astype(jnp.bfloat16)

    p_diag = for_partner(ox, oy)
    p_x = for_partner(ox, y)
    for_own(ox, oy, p_diag)
    a_diag = send(csum.at[ox, oy, 0], ra1.at[oy], to_x)
    b_diag = send(csum.at[ox, oy, 1], rb1.at[ox], to_y)
    p_y = for_partner(x, oy)
    for_own(ox, y, p_x)
    a_x = send(csum.at[ox, y, 0], ra1.at[y], to_x)
    p_own = for_partner(x, y)
    for_own(x, oy, p_y)
    b_y = send(csum.at[x, oy, 1], rb1.at[x], to_y)
    a_diag.wait_recv()
    add(x, oy, 0, ra1.at[oy])
    a_last = send(csum.at[x, oy, 0], ra2, to_y)
    b_diag.wait_recv()
    add(ox, y, 1, rb1.at[ox])
    b_last = send(csum.at[ox, y, 1], rb2, to_x)
    for_own(x, y, p_own)
    a_x.wait_recv()
    b_y.wait_recv()
    a_last.wait_recv()
    b_last.wait_recv()
    for h, first, last in ((0, ra1.at[y], ra2), (1, rb1.at[x], rb2)):
        at = pl.ds(h * half, half)
        total = csum[x, y, h].astype(jnp.float32) + first[...].astype(jnp.float32)
        total = total + last[...].astype(jnp.float32)
        out[:, at] = (total * dn_scale[:, at]).astype(out.dtype)
    for copy in copies:
        copy.wait_send()


def body(hidden_in, norm_gain, up_weight, up_scale, down_weight, down_scale):
    rep, pair = lax.axis_index("rep"), lax.axis_index("fy")
    n = lax.axis_size("fz")
    width = up_weight.shape[1] // 4
    rows, depth = hidden_in.shape
    kr, cols = up_weight.shape[0], down_weight.shape[1]

    wide = hidden_in.astype(jnp.float32)
    normed = (
        wide * lax.rsqrt(jnp.mean(wide * wide, axis=1, keepdims=True) + 1e-06) * norm_gain
    ).astype(jnp.bfloat16)

    def cut(array, dim, yy):
        return lax.dynamic_slice_in_dim(array, (rep * 2 + yy) * width, width, dim)

    low = jnp.bfloat16
    half = depth // 2
    sends = 4 * (n - 1) + 20
    vmem = pl.BlockSpec(memory_space=pltpu.VMEM)
    return pl.pallas_call(
        functools.partial(kernel, n),
        out_shape=jax.ShapeDtypeStruct((rows, depth), low),
        in_specs=[vmem] * 7,
        out_specs=vmem,
        scratch_shapes=[
            pltpu.VMEM((2, 2, 2, rows, depth), low),
            pltpu.VMEM((2 * n * kr, width), low),
            pltpu.VMEM((2 * n, width, cols), low),
            pltpu.VMEM((rows, width), low),
            pltpu.VMEM((2, 2, 2, rows, half), low),
            pltpu.VMEM((2, 2, 2, rows, half), low),
            pltpu.VMEM((2, 2, 2, rows, half), low),
            pltpu.VMEM((2, rows, half), low),
            pltpu.VMEM((2, rows, half), low),
            pltpu.VMEM((rows, half), low),
            pltpu.VMEM((rows, half), low),
            pltpu.SemaphoreType.DMA((sends,)),
            pltpu.SemaphoreType.DMA((sends,)),
            pltpu.SemaphoreType.DMA((3,)),
        ],
        compiler_params=pltpu.CompilerParams(
            collective_id=0, has_side_effects=True, vmem_limit_bytes=60 * 1024 * 1024
        ),
    )(
        normed,
        cut(up_weight, 1, pair).astype(low),
        cut(up_weight, 1, 1 - pair).astype(low),
        cut(down_weight, 0, pair).astype(low),
        cut(down_weight, 0, 1 - pair).astype(low),
        cut(up_scale, 0, pair).reshape(1, width),
        down_scale.reshape(1, depth),
    )


def solution(mesh):
    n_rep, n_fs, n_tp = (mesh.shape[a] for a in ("rep", "fs", "tp"))
    split = Mesh(mesh.devices.reshape(n_rep, n_fs // 2, 2, n_tp), ("rep", "fz", "fy", "tp"))
    fs = ("fz", "fy")
    tokens = P(("rep", *fs, "tp"), None)
    placed = (tokens, P(), P(fs, "tp"), P("tp"), P("tp", fs), P())
    return jax.shard_map(body, mesh=split, in_specs=placed, out_specs=tokens, check_vma=False)
```

time: 398 us -> 232 us (0.58)
  waiting for transfers between devices: 306 us -> 0 us
  Pallas kernels: 0 us -> 219 us
  matrix products: 33.1 us -> 0 us
  blocking collectives: 32.8 us -> 0 us
  between operations: 13.2 us -> 0.01 us
    pallas_call x0 -> x1, Pallas kernels: none -> 219 us  [body(): pl.pallas_call(functools.partial(kernel, n), out_shape=jax.ShapeDtypeStru...]
    all_gather x3 -> x0, waiting for transfers between devices: 213 us -> none  [the longest x1 80.8 us: body(): down_whole = lax.all_gather(down_pair, 'fz', axis=1, tiled=True)]
    reduce_scatter x1 -> x0, waiting for transfers between devices: 92.4 us -> none  [body(): lax.psum_scatter(jnp.dot(act, down_whole, preferred_element_type=jnp.floa...]
    dot_general x1 -> x0, matrix products: 33.1 us -> none  [body(): jnp.dot(act, down_whole, preferred_element_type=jnp.float32)]
    all_to_all x2 -> x0, blocking collectives: 32.8 us -> none  [the longest x1 17.7 us: body(): up_pair = lax.all_to_all(up_low, 'fy', 1, 0, tiled=True)]
  transfers between devices with their start and end apart: 4 -> 0, of which waited for: 4 -> 0; matrix products, arithmetic and copies ran while one was open for 1% -> 0% of each run, Pallas kernels for 0% -> 0%
where the time goes in v2:
time: 232 us
  Pallas kernels  219 us (94%)
  local copies, waits for them, and re-layouts  9.33 us (4%)
  other arithmetic  3.48 us (2%)
    pallas_call x1, Pallas kernels, body(): pl.pallas_call(functools.partial(kernel, n), out_shape=jax.ShapeDtypeStru...  219 us

profile of v2, /device:TPU:0, one launch (start us, length us, event | category | flops | bytes accessed | tf_op | source)
XLA Modules:
  0.0 231.5 jit_solution(747680728499355670)
XLA Ops:
  0.0 0.0 copy-start
  0.0 0.0 copy-start.1
  0.0 1.9 fusion
  1.9 1.3 dynamic_slice.19
  3.2 2.7 %dynamic-slice_convert_fusion.2 = (bf16[256,1024]{1,0:T(8,128)(2,1)}, bf16[256,1024]{1,0:T(8,128)(2,1)}) fusion(f32[256,4096]{1,0:T(8,128)} %param.8, s32[]{:T(128)S(6)} %select_n.10, s32[]{:T(128)S(6)} %select_n.4), kind=kLoop, calls=%fused_computation.7 | loop fusion | bytes 2097160 | tf_op jit(solution)/shard_map/convert_element_type | solution.py:237
  5.9 2.6 %dynamic-slice_convert_fusion = (bf16[1024,256]{1,0:T(8,128)(2,1)}, bf16[1024,256]{1,0:T(8,128)(2,1)}) fusion(f32[4096,256]{1,0:T(8,128)} %param.10, s32[]{:T(128)S(6)} %select_n.10, s32[]{:T(128)S(6)} %select_n.4), kind=kLoop, calls=%fused_computation.5 | loop fusion | bytes 2097160 | tf_op jit(solution)/shard_map/convert_element_type | solution.py:239
  8.5 0.0 copy-done
  8.5 0.0 copy-done.1
  8.5 1.6 fusion.2.normed
  10.1 218.7 %shard_map.64 = bf16[384,2048]{1,0:T(8,128)(2,1)} custom-call(bf16[384,2048]{1,0:T(8,128)(2,1)} %fusion.2.normed, bf16[256,1024]{1,0:T(8,128)(2,1)} %get-tuple-element.8.up_own, bf16[256,1024]{1,0:T(8,128)(2,1)} %get-tuple-element.7.up_peer, bf16[1024,256]{1,0:T(8,128)(2,1)} %get-tuple-element.6.dn_own, bf16[1024,256]{1,0:T(8,128)(2,1)} %get-tuple-element.5.dn_peer, ...), custom_call_target="tpu_custom_call" | custom-call | tf_op jit(solution)/shard_map/pallas_call | solution.py:210
  228.8 2.7 %copy.8 = bf16[384,2048]{1,0:T(8,128)(2,1)} copy(bf16[384,2048]{1,0:T(8,128)(2,1)} %shard_map.64) | data formatting | bytes 3145728
  (1 shorter events, 0.0 us)
Async XLA Ops:
  0.0 8.5 %copy-start = (bf16[384,2048]{1,0:T(8,128)(2,1)S(1)}, bf16[384,2048]{1,0:T(8,128)(2,1)}, u32[]{:S(2)}) copy-start(bf16[384,2048]{1,0:T(8,128)(2,1)} %param.6) | copy-start | bytes 4718596
  0.0 8.5 %copy-start.1 = (f32[2048]{0:T(1024)S(1)}, f32[2048]{0:T(1024)}, u32[]{:S(2)}) copy-start(f32[2048]{0:T(1024)} %param.7) | copy-start | bytes 24580

commit v3 on v1

v3 whole, which is shorter than its diff:
```python
import functools

import jax
import jax.numpy as jnp
from jax import lax
from jax.experimental import pallas as pl
from jax.experimental.pallas import tpu as pltpu
from jax.sharding import Mesh, PartitionSpec as P

MESH = pl.DeviceIdType.MESH


def kernel(
    n, normed, up_own, up_peer, dn_own, dn_peer, up_scale, dn_scale, out,
    tok, up_w, dn_w, act, psend, precv, csum, ra1, rb1, ra2, rb2, ss, rs, ls,
):
    x, z, y, c = (lax.axis_index(a) for a in ("rep", "fz", "fy", "tp"))
    ox, oy, oc = 1 - x, 1 - y, 1 - c
    right, left = lax.rem(z + 1, n), lax.rem(z + n - 1, n)
    to_x, to_y, to_c = {"rep": ox}, {"fy": oy}, {"tp": oc}
    to_right, to_left = {"fz": right}, {"fz": left}
    kr, width = up_own.shape
    rows, depth = normed.shape
    cols = dn_own.shape[1]
    top, part_rows = rows // 2, kr // 2

    barrier = pltpu.get_barrier_semaphore()
    for other in (to_x, to_y, to_c, to_right, to_left):
        pl.semaphore_signal(barrier, inc=1, device_id=other, device_id_type=MESH)
    pl.semaphore_wait(barrier, 5)

    count = [0]

    def send(src, dst, other):
        i = count[0]
        count[0] += 1
        copy = pltpu.make_async_remote_copy(
            src_ref=src, dst_ref=dst, send_sem=ss.at[i], recv_sem=rs.at[i],
            device_id=other, device_id_type=MESH,
        )
        copy.start()
        return copy

    def up_at(zz, yy, h):
        start = (zz * 2 + yy) * kr + h * part_rows
        return up_w.at[pl.ds(pl.multiple_of(start, part_rows), part_rows)]

    ups, downs = {}, {}

    def up_hop(step, yy, chain):
        pair = []
        for h, other in ((0, to_right), (1, to_left)):
            owner = lax.rem(z - step + n, n) if h == 0 else lax.rem(z + step, n)
            dst = up_at(owner, yy, h)
            first = step == 0 and chain == 0
            pair.append(send(up_own.at[pl.ds(h * part_rows, part_rows)] if first else dst, dst, other))
        ups[chain, step] = pair

    def up_arrived(step, chain):
        for copy in ups[chain, step]:
            copy.wait_recv()

    def slots(k):
        return lax.rem(z - k + n, n) * 2, lax.rem(z + k, n) * 2 + 1

    def down_hop(step):
        one, two = (dn_w.at[s] for s in slots(step))
        downs[step] = send(one, one, to_right), send(two, two, to_left)

    up_hop(0, y, 0)
    here = pl.ds(pl.multiple_of((z * 2 + y) * kr, kr), kr)
    y_up = send(up_peer, up_w.at[here], to_y)
    y_dn = send(dn_peer, dn_w.at[z * 2 + y], to_y)
    tx = send(normed, tok.at[c, x, y], to_x)
    ty = send(normed, tok.at[c, x, y], to_y)
    tc = send(normed, tok.at[c, x, y], to_c)
    mine = (
        pltpu.make_async_copy(up_own, up_w.at[here], ls.at[0]),
        pltpu.make_async_copy(dn_own, dn_w.at[z * 2 + y], ls.at[1]),
        pltpu.make_async_copy(normed, tok.at[c, x, y], ls.at[2]),
    )
    for copy in mine:
        copy.start()

    up_arrived(0, 0)
    up_hop(1, y, 0)
    y_up.wait_recv()
    up_hop(0, oy, 1)
    for step in range(1, n - 2):
        up_arrived(step, 0)
        up_hop(step + 1, y, 0)
    up_arrived(0, 1)
    up_hop(1, oy, 1)
    tx.wait_recv()
    diag_y = send(tok.at[c, ox, y, pl.ds(0, top)], tok.at[c, ox, y, pl.ds(0, top)], to_y)
    cx = send(tok.at[c, ox, y], tok.at[c, ox, y], to_c)
    for step in range(1, n - 2):
        up_arrived(step, 1)
        up_hop(step + 1, oy, 1)
    for copy in mine:
        copy.wait()
    y_dn.wait_recv()
    down_hop(0)
    ty.wait_recv()
    diag_x = send(tok.at[c, x, oy, pl.ds(top, top)], tok.at[c, x, oy, pl.ds(top, top)], to_x)
    cy = send(tok.at[c, x, oy], tok.at[c, x, oy], to_c)
    up_arrived(n - 2, 0)
    up_arrived(n - 2, 1)
    diag_y.wait_recv()
    diag_x.wait_recv()
    cd = send(tok.at[c, ox, oy], tok.at[c, ox, oy], to_c)
    for copy in (tc, cx, cy, cd):
        copy.wait_recv()

    tile = min(256, width)

    @pl.loop(0, 8)
    def _(i):
        cc, xx, yy = i // 4, (i // 2) % 2, i % 2

        @pl.loop(0, width // tile)
        def _(j):
            at = pl.ds(pl.multiple_of(j * tile, tile), tile)
            pre = jnp.dot(tok[cc, xx, yy], up_w[:, at], preferred_element_type=jnp.float32)
            act[cc, xx, yy, :, at] = jnp.square(
                jnp.maximum(pre * up_scale[:, at], 0.0)
            ).astype(jnp.bfloat16)

    def each_part(k, cc, emit):
        one, two = slots(k)

        @pl.loop(0, 8)
        def _(i):
            h, f, s = i // 4, (i // 2) % 2, i % 2
            xx, yy = f + h * (s - f), s + h * (f - s)
            part = jnp.dot(
                act[cc, xx, yy], dn_w[one + h * (two - one)], preferred_element_type=jnp.float32
            )
            emit(h, f, s, part.astype(jnp.bfloat16))

    given, first, last = {}, {}, {}

    def for_partner(k):
        p = k % 2
        if k >= 2:
            given[k - 2].wait_send()

        def emit(h, f, s, part):
            psend[p, h, f, s] = part

        each_part(k, oc, emit)
        given[k] = send(psend.at[p], precv.at[k], to_c)

    def for_own(k):
        p = k % 2
        given[k].wait_recv()

        def emit(h, f, s, part):
            total = part.astype(jnp.float32) + precv[k, h, f, s].astype(jnp.float32)
            csum[p, h, f, s] = total.astype(jnp.bfloat16)

        each_part(k, c, emit)
        first[k] = (
            send(csum.at[p, 0, ox], ra1.at[k], to_x),
            send(csum.at[p, 1, oy], rb1.at[k], to_y),
        )

    def second_stage(k):
        p = k % 2
        sent = []
        for h, f, s, got, dst, other in (
            (0, x, oy, ra1, ra2, to_y), (1, y, ox, rb1, rb2, to_x)
        ):
            first[k][h].wait_recv()
            total = csum[p, h, f, s].astype(jnp.float32) + got[k, s].astype(jnp.float32)
            csum[p, h, f, s] = total.astype(jnp.bfloat16)
            sent.append(send(csum.at[p, h, f, s], dst.at[k], other))
        last[k] = sent

    def finish(k):
        p = k % 2
        for h, f, s, one, two in ((0, x, y, ra1, ra2), (1, y, x, rb1, rb2)):
            last[k][h].wait_recv()
            total = csum[p, h, f, s].astype(jnp.float32) + one[k, s].astype(jnp.float32)
            total = total + two[k].astype(jnp.float32)
            slot = slots(k)[h]
            value = (total * dn_scale[slot]).astype(out.dtype)
            if cols % 128 == 0:
                out[:, pl.ds(pl.multiple_of(slot * cols, cols), cols)] = value
            else:
                out[slot] = value
        for copy in (*first[k], *last[k]):
            copy.wait_send()

    for k in range(n):
        if k >= 1:
            for copy in downs[k - 1]:
                copy.wait_recv()
            if k < n - 1:
                down_hop(k)
        for_partner(k)
        if k >= 1:
            second_stage(k - 1)
        if k >= 2:
            finish(k - 2)
        for_own(k)
    second_stage(n - 1)
    finish(n - 2)
    finish(n - 1)
    for pair in (*ups.values(), *downs.values()):
        for copy in pair:
            copy.wait_send()
    for copy in (y_up, y_dn, tx, ty, tc, diag_y, cx, diag_x, cy, cd, given[n - 2], given[n - 1]):
        copy.wait_send()


def body(hidden_in, norm_gain, up_weight, up_scale, down_weight, down_scale):
    rep, pair = lax.axis_index("rep"), lax.axis_index("fy")
    n = lax.axis_size("fz")
    width = up_weight.shape[1] // 4
    rows, depth = hidden_in.shape
    kr, cols = up_weight.shape[0], down_weight.shape[1]

    wide = hidden_in.astype(jnp.float32)
    normed = (
        wide * lax.rsqrt(jnp.mean(wide * wide, axis=1, keepdims=True) + 1e-06) * norm_gain
    ).astype(jnp.bfloat16)

    def cut(array, dim, yy):
        return lax.dynamic_slice_in_dim(array, (rep * 2 + yy) * width, width, dim)

    low = jnp.bfloat16
    sends = 6 * (n - 1) + 10 + 5 * n
    flat = cols % 128 == 0
    vmem = pl.BlockSpec(memory_space=pltpu.VMEM)
    made = pl.pallas_call(
        functools.partial(kernel, n),
        out_shape=jax.ShapeDtypeStruct((rows, depth) if flat else (2 * n, rows, cols), low),
        in_specs=[vmem] * 7,
        out_specs=vmem,
        scratch_shapes=[
            pltpu.VMEM((2, 2, 2, rows, depth), low),
            pltpu.VMEM((2 * n * kr, width), low),
            pltpu.VMEM((2 * n, width, cols), low),
            pltpu.VMEM((2, 2, 2, rows, width), low),
            pltpu.VMEM((2, 2, 2, 2, rows, cols), low),
            pltpu.VMEM((n, 2, 2, 2, rows, cols), low),
            pltpu.VMEM((2, 2, 2, 2, rows, cols), low),
            pltpu.VMEM((n, 2, rows, cols), low),
            pltpu.VMEM((n, 2, rows, cols), low),
            pltpu.VMEM((n, rows, cols), low),
            pltpu.VMEM((n, rows, cols), low),
            pltpu.SemaphoreType.DMA((sends,)),
            pltpu.SemaphoreType.DMA((sends,)),
            pltpu.SemaphoreType.DMA((3,)),
        ],
        compiler_params=pltpu.CompilerParams(
            collective_id=0, has_side_effects=True, vmem_limit_bytes=60 * 1024 * 1024
        ),
    )(
        normed,
        cut(up_weight, 1, pair).astype(low),
        cut(up_weight, 1, 1 - pair).astype(low),
        cut(down_weight, 0, pair).astype(low),
        cut(down_weight, 0, 1 - pair).astype(low),
        cut(up_scale, 0, pair).reshape(1, width),
        down_scale.reshape(2 * n, 1, cols),
    )
    return made if flat else made.transpose(1, 0, 2).reshape(rows, depth)


def solution(mesh):
    n_rep, n_fs, n_tp = (mesh.shape[a] for a in ("rep", "fs", "tp"))
    split = Mesh(mesh.devices.reshape(n_rep, n_fs // 2, 2, n_tp), ("rep", "fz", "fy", "tp"))
    fs = ("fz", "fy")
    tokens = P(("rep", *fs, "tp"), None)
    placed = (tokens, P(), P(fs, "tp"), P("tp"), P("tp", fs), P())
    return jax.shard_map(body, mesh=split, in_specs=placed, out_specs=tokens, check_vma=False)
```

time: 398 us -> 201 us (0.51)
  waiting for transfers between devices: 306 us -> 0 us
  Pallas kernels: 0 us -> 188 us
  matrix products: 33.1 us -> 0 us
  blocking collectives: 32.8 us -> 0 us
  between operations: 13.2 us -> 0.01 us
    all_gather x3 -> x0, waiting for transfers between devices: 213 us -> none  [the longest x1 80.8 us: body(): down_whole = lax.all_gather(down_pair, 'fz', axis=1, tiled=True)]
    pallas_call x0 -> x1, Pallas kernels: none -> 188 us  [body(): pl.pallas_call(functools.partial(kernel, n), out_shape=jax.ShapeDtypeStru...]
    reduce_scatter x1 -> x0, waiting for transfers between devices: 92.4 us -> none  [body(): lax.psum_scatter(jnp.dot(act, down_whole, preferred_element_type=jnp.floa...]
    dot_general x1 -> x0, matrix products: 33.1 us -> none  [body(): jnp.dot(act, down_whole, preferred_element_type=jnp.float32)]
    all_to_all x2 -> x0, blocking collectives: 32.8 us -> none  [the longest x1 17.7 us: body(): up_pair = lax.all_to_all(up_low, 'fy', 1, 0, tiled=True)]
  transfers between devices with their start and end apart: 4 -> 0, of which waited for: 4 -> 0; matrix products, arithmetic and copies ran while one was open for 1% -> 0% of each run, Pallas kernels for 0% -> 0%
where the time goes in v3:
time: 201 us
  Pallas kernels  188 us (94%)
  local copies, waits for them, and re-layouts  9.33 us (5%)
  other arithmetic  3.48 us (2%)
    pallas_call x1, Pallas kernels, body(): pl.pallas_call(functools.partial(kernel, n), out_shape=jax.ShapeDtypeStru...  188 us

profile of v3, /device:TPU:0, one launch (start us, length us, event | category | flops | bytes accessed | tf_op | source)
XLA Modules:
  0.0 200.6 jit_solution(3867213394650608687)
XLA Ops:
  0.0 0.0 copy-start
  0.0 0.0 copy-start.1
  0.0 1.9 fusion
  1.9 1.3 dynamic_slice.19
  3.2 2.7 %dynamic-slice_convert_fusion.2 = (bf16[256,1024]{1,0:T(8,128)(2,1)}, bf16[256,1024]{1,0:T(8,128)(2,1)}) fusion(f32[256,4096]{1,0:T(8,128)} %param.8, s32[]{:T(128)S(6)} %select_n.10, s32[]{:T(128)S(6)} %select_n.4), kind=kLoop, calls=%fused_computation.7 | loop fusion | bytes 2097160 | tf_op jit(solution)/shard_map/convert_element_type | solution.py:263
  5.9 2.6 %dynamic-slice_convert_fusion = (bf16[1024,256]{1,0:T(8,128)(2,1)}, bf16[1024,256]{1,0:T(8,128)(2,1)}) fusion(f32[4096,256]{1,0:T(8,128)} %param.10, s32[]{:T(128)S(6)} %select_n.10, s32[]{:T(128)S(6)} %select_n.4), kind=kLoop, calls=%fused_computation.5 | loop fusion | bytes 2097160 | tf_op jit(solution)/shard_map/convert_element_type | solution.py:265
  8.5 0.0 copy-done
  8.5 0.0 copy-done.1
  8.5 1.6 fusion.2.normed
  10.1 187.8 %shard_map.64 = bf16[384,2048]{1,0:T(8,128)(2,1)} custom-call(bf16[384,2048]{1,0:T(8,128)(2,1)} %fusion.2.normed, bf16[256,1024]{1,0:T(8,128)(2,1)} %get-tuple-element.8.up_own, bf16[256,1024]{1,0:T(8,128)(2,1)} %get-tuple-element.7.up_peer, bf16[1024,256]{1,0:T(8,128)(2,1)} %get-tuple-element.6.dn_own, bf16[1024,256]{1,0:T(8,128)(2,1)} %get-tuple-element.5.dn_peer, ...), custom_call_target="tpu_custom_call" | custom-call | tf_op jit(solution)/shard_map/pallas_call | solution.py:236
  197.9 2.7 %copy.8 = bf16[384,2048]{1,0:T(8,128)(2,1)} copy(bf16[384,2048]{1,0:T(8,128)(2,1)} %shard_map.64) | data formatting | bytes 3145728
  (1 shorter events, 0.0 us)
Async XLA Ops:
  0.0 8.5 %copy-start = (bf16[384,2048]{1,0:T(8,128)(2,1)S(1)}, bf16[384,2048]{1,0:T(8,128)(2,1)}, u32[]{:S(2)}) copy-start(bf16[384,2048]{1,0:T(8,128)(2,1)} %param.6) | copy-start | bytes 4718596
  0.0 8.5 %copy-start.1 = (f32[2048]{0:T(1024)S(1)}, f32[2048]{0:T(1024)}, u32[]{:S(2)}) copy-start(f32[2048]{0:T(1024)} %param.7) | copy-start | bytes 24580
